TPU v7x, 32 devices: a whole 2x2x4 slice. The times are simulated.
32 devices in a mesh: ep: 8 (over z, x), tp: 4 (over y, core).
Axes of the slice: x: 2, y: 2, z: 4, core: 2. Of those that a mesh axis runs over, the one named last changes fastest.
Arguments:
- tokens: bfloat16 [1024, 1024], P('ep', 'tp'), may hold values from -6 to 6
- cotangent: bfloat16 [1024, 1024], P('ep', 'tp'), may hold values from -4 to 4
- routes: int32 [1024, 2], P('ep'), may hold values from 0 to 7, all different within a row; in each aligned block of 128 rows (0 to 127, 128 to 255, ...) at most 40 rows name the same one
- route_weights: bfloat16 [1024, 2], P('ep'), may hold values from 0.099609375 to 0.8984375
- w_gate: bfloat16 [8, 1024, 2816], P('ep', None, 'tp'), may hold values from -0.1875 to 0.1875
- w_up: bfloat16 [8, 1024, 2816], P('ep', None, 'tp'), may hold values from -0.1875 to 0.1875
- w_down: bfloat16 [8, 2816, 1024], P('ep', 'tp'), may hold values from -0.109375 to 0.109375
- dense_weight: bfloat16 [1024, 1024], P('tp', 'ep'), may hold values from -0.25 to 0.25
- mix_gate: float32 [1024], replicated, may hold values from 0.1 to 1.9
Outputs:
- token_grad: bfloat16 [1024, 1024], P('ep', 'tp')
- route_grad: float32 [1024, 2], P('ep')
- gate_grad: bfloat16 [8, 1024, 2816], P('ep', None, 'tp')
- up_grad: bfloat16 [8, 1024, 2816], P('ep', None, 'tp')
- down_grad: bfloat16 [8, 2816, 1024], P('ep', 'tp')
- dense_grad: float32 [1024, 1024], P('tp', 'ep')
- mix_grad: float32 [1024], replicated
Inputs may be any that keep to these rules, and one draw needn't show every extreme that they name: `routes`: each row names 2 different experts. In the rows of one index of ep (aligned blocks of 128 rows) no expert is named by more than 40 rows, a bound that some block reaches.
All inputs are finite; a program needn't handle non-finite values.
Results may differ from a plain program's by a relative error of at most 0.0065.
Values may be sent and summed in bfloat16 or wider, within the bound.
A program may use at most 64 MiB of HBM per device.

v0:
```python
import jax
import jax.numpy as jnp
from jax import lax
from jax.sharding import PartitionSpec as P

FF = 2816
BF = jnp.bfloat16
F32 = jnp.float32


def spread(values, group_size):
    experts = values.shape[0]
    copies = jnp.broadcast_to(values[:, None], (experts, group_size) + values.shape[1:])
    return copies.reshape((experts * group_size,) + values.shape[1:])


def swap(values, axis):
    return lax.all_to_all(values, axis, split_axis=0, concat_axis=0, tiled=True)


def local(tokens, cotangent, routes, route_weights, w_gate, w_up, w_down, dense_weight, mix_gate):
    tp_count = lax.axis_size("tp")
    ep_count = lax.axis_size("ep")
    slice_width = w_gate.shape[2]
    group_size = FF // (slice_width * tp_count)
    experts = ep_count // group_size
    token_count, top_count = routes.shape
    width_part = tokens.shape[1]
    width = width_part * tp_count
    capacity = 5 * token_count * top_count // (4 * experts)
    slots = experts * capacity
    rows_here = ep_count * capacity
    expert_ids = jnp.arange(experts, dtype=jnp.int32)
    named = routes[:, :, None] == expert_ids[None, None, :]
    member = jnp.any(named, axis=1)
    token_ids = jnp.arange(token_count, dtype=jnp.int32)
    before = (token_ids[:, None] > token_ids[None, :]).astype(BF)
    rank = jnp.dot(before, member.astype(BF), preferred_element_type=F32)
    weight_of = jnp.sum(jnp.where(named, route_weights.astype(F32)[:, :, None], 0.0), axis=1)
    slot_ids = jnp.arange(capacity, dtype=jnp.int32).astype(F32)
    rank_t = jnp.where(member, rank, -1.0).T
    hit = rank_t[:, None, :] == slot_ids[None, :, None]
    dispatch = hit.astype(BF).reshape(slots, token_count)
    slot_weight = jnp.sum(jnp.where(hit, weight_of.T[:, None, :], 0.0), axis=2).astype(BF)

    def pick(values):
        taken = jnp.dot(dispatch, values, preferred_element_type=F32).astype(BF)
        return spread(taken.reshape(experts, capacity, values.shape[1]), group_size)

    rows_part = swap(pick(tokens), "ep")
    grads_full = lax.all_gather(cotangent, "tp", axis=1, tiled=True)
    lanes = jnp.broadcast_to(spread(slot_weight, group_size)[:, :, None], (ep_count, capacity, 128))
    arrived = swap(jnp.concatenate([pick(grads_full), lanes], axis=2), "ep")
    arrived = arrived.reshape(rows_here, width + 128)
    grads_in, weight_col = (arrived[:, :width], arrived[:, width : width + 1].astype(F32))
    rows_in = lax.all_gather(rows_part.reshape(rows_here, width_part), "tp", axis=1, tiled=True)
    contract_rows = (((0,), (0,)), ((), ()))
    contract_cols = (((1,), (1,)), ((), ()))
    dense_cols = dense_weight.shape[1]
    scaled = (mix_gate[None, :] * grads_full.astype(F32)).astype(BF)
    product = lax.dot_general(tokens, scaled, contract_rows, preferred_element_type=F32).astype(BF)
    product = product.reshape(width_part, ep_count, dense_cols).transpose(1, 0, 2)
    copies = jnp.broadcast_to(dense_weight[None], (ep_count,) + dense_weight.shape)
    outgoing, _ = lax.optimization_barrier((jnp.concatenate([copies, product], axis=1), arrived))
    met = swap(outgoing, "ep")
    gathered, shares = (met[:, :width_part], met[:, width_part:])
    dense_grad = jnp.sum(shares.astype(F32), axis=0) * (1.0 / ep_count)
    gate_matrix = w_gate[0]
    up_matrix = w_up[0]
    down_matrix = w_down[0]
    pre_gate = jnp.dot(rows_in, gate_matrix, preferred_element_type=F32)
    pre_up = jnp.dot(rows_in, up_matrix, preferred_element_type=F32)
    sigmoid_gate = jax.nn.sigmoid(pre_gate)
    activated = pre_gate * sigmoid_gate
    hidden = activated * pre_up
    hidden_bf = hidden.astype(BF)
    projected = lax.dot_general(grads_in, down_matrix, contract_cols, preferred_element_type=F32)
    route_part = jnp.sum(hidden_bf.astype(F32) * projected, axis=1)
    hidden_grad = weight_col * projected
    d_gate = (hidden_grad * pre_up * sigmoid_gate * (1.0 + pre_gate * (1.0 - sigmoid_gate))).astype(
        BF
    )
    d_up = (hidden_grad * activated).astype(BF)
    weighted = (weight_col * hidden).astype(BF)
    partial_value = (
        lax.dot_general(d_gate, gate_matrix, contract_cols, preferred_element_type=F32)
        + lax.dot_general(d_up, up_matrix, contract_cols, preferred_element_type=F32)
    ).astype(BF)
    mixed = lax.all_to_all(partial_value, "tp", split_axis=1, concat_axis=0, tiled=True)
    column_sum = jnp.sum(mixed.reshape(tp_count, rows_here, -1).astype(F32), axis=0).astype(BF)
    returned = swap(column_sum.reshape(ep_count, capacity, width_part), "ep")
    moment = lax.dot_general(tokens, grads_full, contract_rows, preferred_element_type=F32)
    moment = moment.reshape(width_part, ep_count, dense_cols)
    gain = jnp.sum(gathered.astype(F32) * moment.transpose(1, 0, 2), axis=1).reshape(1, width)
    gain, route_part, _ = lax.optimization_barrier((gain, route_part, mixed))
    devices = ep_count * tp_count
    route_rows = jnp.broadcast_to(
        route_part.reshape(ep_count, 1, capacity), (ep_count, tp_count, capacity)
    ).reshape(devices, capacity)
    packed = jnp.concatenate([jnp.broadcast_to(gain, (devices, width)), route_rows], axis=1)
    small = swap(packed[:, None, :], ("ep", "tp")).reshape(devices, width + capacity)
    mix_grad = jnp.sum(small[:, :width], axis=0) * (1.0 / ep_count)
    slot_route = jnp.sum(small[:, width:].reshape(experts, group_size * tp_count, capacity), axis=1)
    expert_route = jnp.sum(jnp.where(hit, slot_route[:, :, None], 0.0), axis=1).T
    route_grad = jnp.sum(jnp.where(named, expert_route[:, None, :], 0.0), axis=2)
    gate_grad = lax.dot_general(rows_in, d_gate, contract_rows, preferred_element_type=F32)
    up_grad = lax.dot_general(rows_in, d_up, contract_rows, preferred_element_type=F32)
    down_grad = lax.dot_general(weighted, grads_in, contract_rows, preferred_element_type=F32)
    back = returned.reshape(experts, group_size, capacity, width_part)
    combine = jnp.broadcast_to(hit[:, None], (experts, group_size) + hit.shape[1:]).astype(BF)
    expert_grad = lax.dot_general(
        combine.reshape(rows_here, token_count),
        back.reshape(rows_here, width_part),
        contract_rows,
        preferred_element_type=F32,
    )
    whole_weight = gathered.transpose(1, 0, 2).reshape(width_part, width)
    dense_dx = lax.dot_general(scaled, whole_weight, contract_cols, preferred_element_type=F32)
    token_grad = (expert_grad + dense_dx).astype(BF)
    return (
        token_grad,
        route_grad,
        gate_grad.astype(BF)[None],
        up_grad.astype(BF)[None],
        down_grad.astype(BF)[None],
        dense_grad,
        mix_grad,
    )


def solution(mesh):
    return jax.shard_map(
        local,
        mesh=mesh,
        in_specs=(
            P("ep", "tp"),
            P("ep", "tp"),
            P("ep", None),
            P("ep", None),
            P("ep", None, "tp"),
            P("ep", None, "tp"),
            P("ep", "tp", None),
            P("tp", "ep"),
            P(),
        ),
        out_specs=(
            P("ep", "tp"),
            P("ep", None),
            P("ep", None, "tp"),
            P("ep", None, "tp"),
            P("ep", "tp", None),
            P("tp", "ep"),
            P(),
        ),
        check_vma=False,
    )
```

profile of v0, /device:TPU:0, one launch (start us, length us, event | category | flops | bytes accessed | tf_op | source)
XLA Modules:
  0.0 121.8 jit_solution(18386872155913374480)
XLA Ops:
  0.6 0.0 copy-start
  0.7 0.1 eq.45
  0.7 0.8 fusion.46
  1.5 0.1 convolution_select_fusion
  1.7 0.1 bitcast_compare_fusion
  1.8 1.7 %convolution_convert_fusion.5 = bf16[320,256]{1,0:T(8,128)(2,1)} fusion(pred[320,128]{1,0:T(32,128)(4,1)S(1)} %bitcast_compare_fusion, bf16[128,256]{1,0:T(8,128)(2,1)} %param.9), kind=kOutput, calls=%fused_computation.20 | convolution fusion | flops 21053440 | bytes 270336 | tf_op jit(solution)/shard_map/dot_general | solution.py:47
  3.5 7.3 %all-to-all-start.1 = ((bf16[8,40,256]{2,1,0:T(8,128)(2,1)}), bf16[8,40,256]{2,1,0:T(8,128)(2,1)S(1)}, u32[]{:S(2)}, u32[]{:S(2)}) async-start(bf16[8,40,256]{2,1,0:T(8,128)(2,1)} %bitcast.6), calls=%async_computation.1 | async-start | bytes 327680 | tf_op jit(solution)/shard_map/all_to_all | solution.py:18
  10.8 0.7 convert_element_type.82
  11.4 0.7 select_reduce_fusion.1
  12.1 6.0 %all_gather.6 = bf16[128,1024]{1,0:T(8,128)(2,1)S(1)} all-gather(bf16[128,256]{1,0:T(8,128)(2,1)} %param.10), channel_id=1, replica_groups=mesh['ep'=8,'tp'=4] {'tp'}, dimensions={1}, use_global_device_ids=true | all-gather | bytes 327680 | tf_op jit(solution)/shard_map/all_gather | solution.py:51
  18.1 0.3 convolution_convert_fusion.3
  18.4 0.2 fusion.27
  18.6 0.9 pad_maximum_fusion.1
  19.5 0.0 all-to-all-done.1
  19.5 6.1 %all-to-all-start = ((bf16[8,40,1152]{2,1,0:T(8,128)(2,1)}), bf16[8,40,1152]{2,1,0:T(8,128)(2,1)}, u32[]{:S(2)}, u32[]{:S(2)}) async-start(bf16[8,40,1152]{2,1,0:T(8,128)(2,1)} %pad_maximum_fusion.1), calls=%async_computation | async-start | bytes 1474560 | tf_op jit(solution)/shard_map/all_to_all | solution.py:18
  25.7 7.9 %all_gather.7 = bf16[320,1024]{1,0:T(8,128)(2,1)S(1)} all-gather(bf16[320,256]{1,0:T(8,128)(2,1)S(1)} %bitcast.83), channel_id=1, replica_groups=mesh['ep'=8,'tp'=4] {'tp'}, dimensions={1}, use_global_device_ids=true | all-gather | bytes 819200 | tf_op jit(solution)/shard_map/all_gather | solution.py:56
  33.6 0.0 copy-done.1
  33.6 1.7 %fusion.9 = f32[320,704]{1,0:T(8,128)} fusion(bf16[320,1024]{1,0:T(8,128)(2,1)S(1)} %all_gather.7, bf16[1,1024,704]{1,2,0:T(8,128)(2,1)S(1)} %copy-done.1), kind=kOutput, calls=%fused_computation.12 | convolution fusion | flops 461373440 | bytes 2998272 | tf_op jit(solution)/shard_map/dot_general | solution.py:72
  35.3 0.0 copy-done.2
  35.3 0.0 copy-done
  35.3 1.7 %fusion.5 = f32[320,704]{1,0:T(8,128)} fusion(bf16[320,1024]{1,0:T(8,128)(2,1)S(1)} %all_gather.7, bf16[1,1024,704]{1,2,0:T(8,128)(2,1)S(1)} %copy-done), kind=kOutput, calls=%fused_computation.8 | convolution fusion | flops 461373440 | bytes 2998272 | tf_op jit(solution)/shard_map/dot_general | solution.py:71
  37.0 8.4 %all-to-all-done = bf16[8,40,1152]{2,1,0:T(8,128)(2,1)} async-done(((bf16[8,40,1152]{2,1,0:T(8,128)(2,1)}), bf16[8,40,1152]{2,1,0:T(8,128)(2,1)}, u32[]{:S(2)}, u32[]{:S(2)}) %all-to-all-start) | async-done | bytes 737312 | tf_op jit(solution)/shard_map/all_to_all | solution.py:18
  45.4 1.0 convert_reduce_fusion.1
  46.4 3.3 %multiply_reduce_fusion.1 = (f32[320]{0:T(512)S(1)}, bf16[320,704]{1,0:T(8,128)(2,1)S(1)}, bf16[320,704]{1,0:T(8,128)(2,1)S(1)}) fusion(f32[320,704]{1,0:T(8,128)} %fusion.9, f32[320,704]{1,0:T(8,128)} %fusion.5, f32[320]{0:T(512)S(1)} %convert_reduce_fusion.1, bf16[1,704,1024]{2,1,0:T(8,128)(2,1)} %param.15, bf16[320,1152]{1,0:T(8,128)(2,1)} %bitcast.4), kind=kOutput, calls=%fused_computation.29 | convolution fusion | flops 465653440 | bytes 4966912 | tf_op jit(solution)/shard_map/dot_general | solution.py:77
  49.7 0.0 copy-start.7
  49.7 0.7 fusion.3
  50.4 0.1 copy-done.14
  50.5 0.2 copy-done.7
  50.6 0.7 fusion.16
  51.3 0.0 copy-start.9
  51.3 0.9 copy.45
  52.2 3.6 %all-to-all-start.2 = ((bf16[320,4,256]{2,0,1:T(8,128)(2,1)}), bf16[320,4,256]{2,0,1:T(8,128)(2,1)S(1)}, u32[]{:S(2)}, u32[]{:S(2)}) async-start(bf16[320,4,256]{2,0,1:T(8,128)(2,1)} %bitcast.76), calls=%async_computation.2 | async-start | bytes 1310720 | tf_op jit(solution)/shard_map/all_to_all | solution.py:89
  55.9 0.0 copy-done.9
  55.9 0.1 copy.37
  56.0 10.1 %all-to-all-done.2 = bf16[320,4,256]{2,0,1:T(8,128)(2,1)S(1)} async-done(((bf16[320,4,256]{2,0,1:T(8,128)(2,1)}), bf16[320,4,256]{2,0,1:T(8,128)(2,1)S(1)}, u32[]{:S(2)}, u32[]{:S(2)}) %all-to-all-start.2) | async-done | bytes 655392 | tf_op jit(solution)/shard_map/all_to_all | solution.py:89
  66.0 0.8 reduce_sum.95
  66.8 3.6 %all-to-all-start.3 = ((bf16[8,40,256]{2,1,0:T(8,128)(2,1)}), bf16[8,40,256]{2,1,0:T(8,128)(2,1)S(1)}, u32[]{:S(2)}, u32[]{:S(2)}) async-start(bf16[8,40,256]{2,1,0:T(8,128)(2,1)} %bitcast.10), calls=%async_computation.3 | async-start | bytes 327680 | tf_op jit(solution)/shard_map/all_to_all | solution.py:18
  70.5 0.0 copy-done.6
  70.5 0.0 copy-done.10
  70.5 0.3 convolution_convert_fusion.4
  70.9 1.1 pad_maximum_fusion
  71.9 6.1 %all-to-all-done.3 = bf16[8,40,256]{2,1,0:T(8,128)(2,1)S(1)} async-done(((bf16[8,40,256]{2,1,0:T(8,128)(2,1)}), bf16[8,40,256]{2,1,0:T(8,128)(2,1)S(1)}, u32[]{:S(2)}, u32[]{:S(2)}) %all-to-all-start.3) | async-done | bytes 163872 | tf_op jit(solution)/shard_map/all_to_all | solution.py:18
  78.0 0.7 copy-done.4
  78.7 3.6 %all-to-all-start.4 = ((bf16[8,512,128]{1,2,0:T(8,128)(2,1)}), bf16[8,512,128]{1,2,0:T(8,128)(2,1)S(1)}, u32[]{:S(2)}, u32[]{:S(2)}) async-start(bf16[8,512,128]{1,2,0:T(8,128)(2,1)} %pad_maximum_fusion), calls=%async_computation.4 | async-start | bytes 2097152 | tf_op jit(solution)/shard_map/all_to_all | solution.py:18
  82.2 1.4 %fusion.55 = f32[256,1024]{0,1:T(8,128)} fusion(bf16[128,256]{1,0:T(8,128)(2,1)S(1)} %copy-done.6, bf16[128,1024]{1,0:T(8,128)(2,1)S(1)} %all_gather.6), kind=kOutput, calls=%fused_computation.84 | convolution fusion | flops 67108864 | bytes 1376256 | tf_op jit(solution)/shard_map/reshape | solution.py:93
  83.6 0.0 copy-done.3
  83.6 3.2 %fusion = bf16[1,1024,704]{1,2,0:T(8,128)(2,1)} fusion(bf16[320,1024]{1,0:T(8,128)(2,1)S(1)} %copy-done.3, bf16[320,704]{1,0:T(8,128)(2,1)} %copy-done.14), kind=kOutput, calls=%fused_computation.3 | convolution fusion | flops 462094336 | bytes 2547712 | tf_op jit(solution)/shard_map/dot_general | solution.py:106
  86.8 0.0 copy-done.8
  86.8 2.1 %fusion.1 = bf16[1,1024,704]{1,2,0:T(8,128)(2,1)} fusion(bf16[320,1024]{1,0:T(8,128)(2,1)S(1)} %copy-done.3, bf16[320,704]{1,0:T(8,128)(2,1)S(1)} %copy-done.8), kind=kOutput, calls=%fused_computation.4 | convolution fusion | flops 462094336 | bytes 2547712 | tf_op jit(solution)/shard_map/dot_general | solution.py:107
  88.9 3.3 %fusion.2 = bf16[1,704,1024]{2,1,0:T(8,128)(2,1)} fusion(bf16[320,1152]{1,0:T(8,128)(2,1)} %bitcast.4, f32[320]{0:T(512)S(1)} %convert_reduce_fusion.1, f32[320,704]{1,0:T(8,128)S(1)} %copy-done.12, f32[320,704]{1,0:T(8,128)S(1)} %copy-done.13), kind=kOutput, calls=%fused_computation.5 | convolution fusion | flops 463671296 | bytes 3900672 | tf_op jit(solution)/shard_map/dot_general | solution.py:108
  92.2 0.3 convolution_bitcast_fusion
  92.5 14.3 %all-to-all-done.4 = bf16[8,512,128]{1,2,0:T(8,128)(2,1)S(1)} async-done(((bf16[8,512,128]{1,2,0:T(8,128)(2,1)}), bf16[8,512,128]{1,2,0:T(8,128)(2,1)S(1)}, u32[]{:S(2)}, u32[]{:S(2)}) %all-to-all-start.4) | async-done | bytes 1048608 | tf_op jit(solution)/shard_map/all_to_all | solution.py:18
  106.8 1.5 %convert_reduce_fusion = (f32[256,128]{0,1:T(8,128)S(1)}, f32[8,128]{1,0:T(8,128)S(1)}) fusion(bf16[8,512,128]{1,2,0:T(8,128)(2,1)S(1)} %all-to-all-done.4, f32[8,256,128]{1,2,0:T(8,128)} %bitcast.78), kind=kLoop, calls=%fused_computation.26 | loop fusion | flops 1276928 | bytes 2232320 | tf_op jit(solution)/shard_map/reduce_sum | solution.py:67
  108.3 0.1 broadcast_in_dim.106
  108.4 0.8 broadcast_in_dim.108
  109.1 2.9 %all-to-all-start.5 = ((f32[32,1,1064]{2,1,0:T(1,128)}), f32[32,1,1064]{2,1,0:T(1,128)S(1)}, u32[]{:S(2)}, u32[]{:S(2)}) async-start(f32[32,1,1064]{2,1,0:T(1,128)} %broadcast_in_dim.108), calls=%async_computation.5 | async-start | bytes 294912 | tf_op jit(solution)/shard_map/all_to_all | solution.py:18
  112.0 0.0 copy-start.11
  112.1 0.8 copy.39
  112.9 0.9 fusion.19
  113.7 6.7 %all-to-all-done.5 = f32[32,1,1064]{2,1,0:T(1,128)S(1)} async-done(((f32[32,1,1064]{2,1,0:T(1,128)}), f32[32,1,1064]{2,1,0:T(1,128)S(1)}, u32[]{:S(2)}, u32[]{:S(2)}) %all-to-all-start.5) | async-done | bytes 136224 | tf_op jit(solution)/shard_map/all_to_all | solution.py:18
  120.5 0.1 fusion.29
  120.6 0.0 copy-done.11
  120.7 0.6 select_reduce_fusion
  121.2 0.6 broadcast_multiply_fusion.1
  (26 shorter events, 0.2 us)
Async XLA Ops:
  0.6 34.6 %copy-start = (bf16[1,1024,704]{1,2,0:T(8,128)(2,1)S(1)}, bf16[1,1024,704]{1,2,0:T(8,128)(2,1)}, u32[]{:S(2)}) copy-start(bf16[1,1024,704]{1,2,0:T(8,128)(2,1)} %param.13) | copy-start | bytes 4325380
  3.5 16.0 %all-to-all-start.1 = ((bf16[8,40,256]{2,1,0:T(8,128)(2,1)}), bf16[8,40,256]{2,1,0:T(8,128)(2,1)S(1)}, u32[]{:S(2)}, u32[]{:S(2)}) async-start(bf16[8,40,256]{2,1,0:T(8,128)(2,1)} %bitcast.6), calls=%async_computation.1 | async-start | bytes 327680 | tf_op jit(solution)/shard_map/all_to_all | solution.py:18
  19.5 14.0 %copy-start.1 = (bf16[1,1024,704]{1,2,0:T(8,128)(2,1)S(1)}, bf16[1,1024,704]{1,2,0:T(8,128)(2,1)}, u32[]{:S(2)}) copy-start(bf16[1,1024,704]{1,2,0:T(8,128)(2,1)} %param.14) | copy-start | bytes 4325380
  19.5 25.8 %all-to-all-start = ((bf16[8,40,1152]{2,1,0:T(8,128)(2,1)}), bf16[8,40,1152]{2,1,0:T(8,128)(2,1)}, u32[]{:S(2)}, u32[]{:S(2)}) async-start(bf16[8,40,1152]{2,1,0:T(8,128)(2,1)} %pad_maximum_fusion.1), calls=%async_computation | async-start | bytes 1474560 | tf_op jit(solution)/shard_map/all_to_all | solution.py:18
  33.6 1.7 %copy-start.2 = (bf16[320,1024]{1,0:T(8,128)(2,1)}, bf16[320,1024]{1,0:T(8,128)(2,1)S(1)}, u32[]{:S(2)}) copy-start(bf16[320,1024]{1,0:T(8,128)(2,1)S(1)} %all_gather.7) | copy-start | bytes 1966084
  49.7 0.8 copy-start.14
  49.7 1.0 copy-start.7
  51.3 4.5 %copy-start.9 = (bf16[256,128]{1,0:T(8,128)(2,1)S(1)}, bf16[256,128]{1,0:T(8,128)(2,1)}, u32[]{:S(2)}) copy-start(bf16[256,128]{1,0:T(8,128)(2,1)} %param.16) | copy-start | bytes 196612
  52.2 18.2 %copy-start.6 = (bf16[128,256]{1,0:T(8,128)(2,1)S(1)}, bf16[128,256]{1,0:T(8,128)(2,1)}, u32[]{:S(2)}) copy-start(bf16[128,256]{1,0:T(8,128)(2,1)} %param.9) | copy-start | bytes 196612
  52.2 18.2 %copy-start.10 = (f32[1024]{0:T(1024)S(1)}, f32[1024]{0:T(1024)}, u32[]{:S(2)}) copy-start(f32[1024]{0:T(1024)} %param.17) | copy-start | bytes 12292
  52.2 13.8 %all-to-all-start.2 = ((bf16[320,4,256]{2,0,1:T(8,128)(2,1)}), bf16[320,4,256]{2,0,1:T(8,128)(2,1)S(1)}, u32[]{:S(2)}, u32[]{:S(2)}) async-start(bf16[320,4,256]{2,0,1:T(8,128)(2,1)} %bitcast.76), calls=%async_computation.2 | async-start | bytes 1310720 | tf_op jit(solution)/shard_map/all_to_all | solution.py:89
  66.8 11.2 %all-to-all-start.3 = ((bf16[8,40,256]{2,1,0:T(8,128)(2,1)}), bf16[8,40,256]{2,1,0:T(8,128)(2,1)S(1)}, u32[]{:S(2)}, u32[]{:S(2)}) async-start(bf16[8,40,256]{2,1,0:T(8,128)(2,1)} %bitcast.10), calls=%async_computation.3 | async-start | bytes 327680 | tf_op jit(solution)/shard_map/all_to_all | solution.py:18
  71.9 11.7 %copy-start.3 = (bf16[320,1024]{1,0:T(8,128)(2,1)S(1)}, bf16[320,1024]{1,0:T(8,128)(2,1)}, u32[]{:S(2)}) copy-start(bf16[320,1024]{1,0:T(8,128)(2,1)} %copy-done.2) | copy-start | bytes 1966084
  78.0 0.7 copy-start.4
  78.7 28.1 %all-to-all-start.4 = ((bf16[8,512,128]{1,2,0:T(8,128)(2,1)}), bf16[8,512,128]{1,2,0:T(8,128)(2,1)S(1)}, u32[]{:S(2)}, u32[]{:S(2)}) async-start(bf16[8,512,128]{1,2,0:T(8,128)(2,1)} %pad_maximum_fusion), calls=%async_computation.4 | async-start | bytes 2097152 | tf_op jit(solution)/shard_map/all_to_all | solution.py:18
  83.6 3.2 %copy-start.8 = (bf16[320,704]{1,0:T(8,128)(2,1)S(1)}, bf16[320,704]{1,0:T(8,128)(2,1)}, u32[]{:S(2)}) copy-start(bf16[320,704]{1,0:T(8,128)(2,1)} %copy-done.7) | copy-start | bytes 1351684
  86.8 2.1 %copy-start.12 = (f32[320,704]{1,0:T(8,128)S(1)}, f32[320,704]{1,0:T(8,128)}, u32[]{:S(2)}) copy-start(f32[320,704]{1,0:T(8,128)} %fusion.9) | copy-start | bytes 2703364
  86.8 2.1 %copy-start.13 = (f32[320,704]{1,0:T(8,128)S(1)}, f32[320,704]{1,0:T(8,128)}, u32[]{:S(2)}) copy-start(f32[320,704]{1,0:T(8,128)} %fusion.5) | copy-start | bytes 2703364
  88.9 3.3 %copy-start.5 = (bf16[8,40,256]{2,1,0:T(8,128)(2,1)S(1)}, bf16[8,40,256]{2,1,0:T(8,128)(2,1)}, u32[]{:S(2)}) copy-start(bf16[8,40,256]{2,1,0:T(8,128)(2,1)} %copy-done.4) | copy-start | bytes 491524
  109.1 11.3 %all-to-all-start.5 = ((f32[32,1,1064]{2,1,0:T(1,128)}), f32[32,1,1064]{2,1,0:T(1,128)S(1)}, u32[]{:S(2)}, u32[]{:S(2)}) async-start(f32[32,1,1064]{2,1,0:T(1,128)} %broadcast_in_dim.108), calls=%async_computation.5 | async-start | bytes 294912 | tf_op jit(solution)/shard_map/all_to_all | solution.py:18
  112.0 8.6 %copy-start.11 = (s32[128,2]{0,1:T(2,128)S(1)}, s32[128,2]{0,1:T(2,128)}, u32[]{:S(2)}) copy-start(s32[128,2]{0,1:T(2,128)} %param.11) | copy-start | bytes 3076
where the time goes:
time: 123 us; the launch traced here: 122 us
  waiting for transfers between devices  45.5 us (37%)
  starting transfers between devices  27.1 us (22%)
  matrix products  21.6 us (18%)
  blocking collectives  13.9 us (11%)
  other arithmetic  9.05 us (7%)
  local copies, waits for them, and re-layouts  3.72 us (3%)
    all_to_all x5, waiting for transfers between devices, swap(): return lax.all_to_all(values, axis, split_axis=0, concat_axis=0, tiled=True)  35.5 us
    all_to_all x5, starting transfers between devices, swap(): return lax.all_to_all(values, axis, split_axis=0, concat_axis=0, tiled=True)  23.5 us
    all_to_all x1, waiting for transfers between devices, local(): lax.all_to_all(partial_value, 'tp', split_axis=1, concat_axis=0, tiled=True)  10.1 us
    all_gather x1, blocking collectives, local(): lax.all_gather(rows_part.reshape(rows_here, width_part), 'tp', axis=1, ti...  7.9 us
    all_gather x1, blocking collectives, local(): grads_full = lax.all_gather(cotangent, 'tp', axis=1, tiled=True)  5.97 us
    all_to_all x1, starting transfers between devices, local(): lax.all_to_all(partial_value, 'tp', split_axis=1, concat_axis=0, tiled=True)  3.61 us
    dot_general x1, matrix products, local(): lax.dot_general(weighted, grads_in, contract_rows, preferred_element_type...  3.32 us
    dot_general x1, matrix products, local(): lax.dot_general(grads_in, down_matrix, contract_cols, preferred_element_t...  3.28 us
  transfers between devices with their start and end apart: 6, of which 5 were waited for; matrix products, arithmetic and copies ran while one was open for 16% of the time, Pallas kernels for 0%

commit v1 on v0

--- a/solution.py
+++ b/solution.py
@@ -19,6 +19,23 @@
 
 
 def local(tokens, cotangent, routes, route_weights, w_gate, w_up, w_down, dense_weight, mix_gate):
+
+    def manage_racks(target):
+        extra, local_now, q_next = (lax.psum(1, "tp"), lax.axis_index("tp"), target.shape[1])
+        all_blocks = []
+        for j in range(extra):
+            all_blocks.append((j, (j + 1) % extra))
+        parts_out = jnp.zeros((*target.shape[:1], extra * q_next, *target.shape[2:]), target.dtype)
+        current_value = target
+        for i0 in range(extra):
+            n_now = (local_now - i0) % extra
+            parts_out = lax.dynamic_update_slice_in_dim(
+                parts_out, current_value, n_now * q_next, axis=1
+            )
+            if i0 < extra - 1:
+                current_value = lax.ppermute(current_value, axis_name="tp", perm=all_blocks)
+        return parts_out
+
     tp_count = lax.axis_size("tp")
     ep_count = lax.axis_size("ep")
     slice_width = w_gate.shape[2]
@@ -53,7 +70,7 @@
     arrived = swap(jnp.concatenate([pick(grads_full), lanes], axis=2), "ep")
     arrived = arrived.reshape(rows_here, width + 128)
     grads_in, weight_col = (arrived[:, :width], arrived[:, width : width + 1].astype(F32))
-    rows_in = lax.all_gather(rows_part.reshape(rows_here, width_part), "tp", axis=1, tiled=True)
+    rows_in = manage_racks(rows_part.reshape(rows_here, width_part))
     contract_rows = (((0,), (0,)), ((), ()))
     contract_cols = (((1,), (1,)), ((), ()))
     dense_cols = dense_weight.shape[1]

time: 123 us -> 122 us (level)
  blocking collectives: 13.9 us -> 5.97 us
  waiting for transfers between devices: 45.5 us -> 53.3 us
  other arithmetic: 9.05 us -> 7.72 us
    ppermute x0 -> x3, waiting for transfers between devices: none -> 14 us  [manage_racks(): current_value = lax.ppermute(current_value, axis_name='tp', perm=all_blocks)]
    all_gather x1 -> x0, blocking collectives: 7.9 us -> none  [local(): lax.all_gather(rows_part.reshape(rows_here, width_part), 'tp', axis=1, ti...]
    all_to_all x5, waiting for transfers between devices: 35.5 us -> 29.2 us  [swap(): return lax.all_to_all(values, axis, split_axis=0, concat_axis=0, tiled=True)]
  transfers between devices with their start and end apart: 6 -> 9, of which waited for: 5 -> 9; matrix products, arithmetic and copies ran while one was open for 16% -> 15% of each run, Pallas kernels for 0% -> 0%
where the time goes in v1:
time: 122 us; the launch traced here: 121 us
  waiting for transfers between devices  53.3 us (44%)
  starting transfers between devices  27.3 us (22%)
  matrix products  21.6 us (18%)
  other arithmetic  7.72 us (6%)
  blocking collectives  5.97 us (5%)
  local copies, waits for them, and re-layouts  3.86 us (3%)
    all_to_all x5, waiting for transfers between devices, swap(): return lax.all_to_all(values, axis, split_axis=0, concat_axis=0, tiled=True)  29.2 us
    all_to_all x5, starting transfers between devices, swap(): return lax.all_to_all(values, axis, split_axis=0, concat_axis=0, tiled=True)  23.6 us
    ppermute x3, waiting for transfers between devices, manage_racks(): current_value = lax.ppermute(current_value, axis_name='tp', perm=all_blocks)  14 us
    all_to_all x1, waiting for transfers between devices, local(): lax.all_to_all(partial_value, 'tp', split_axis=1, concat_axis=0, tiled=True)  10.1 us
    all_gather x1, blocking collectives, local(): grads_full = lax.all_gather(cotangent, 'tp', axis=1, tiled=True)  5.97 us
    all_to_all x1, starting transfers between devices, local(): lax.all_to_all(partial_value, 'tp', split_axis=1, concat_axis=0, tiled=True)  3.61 us
    dot_general x1, matrix products, local(): lax.dot_general(weighted, grads_in, contract_rows, preferred_element_type...  3.32 us
    dot_general x1, matrix products, local(): lax.dot_general(grads_in, down_matrix, contract_cols, preferred_element_t...  3.28 us
  transfers between devices with their start and end apart: 9, of which 9 were waited for; matrix products, arithmetic and copies ran while one was open for 15% of the time, Pallas kernels for 0%

profile of v1, /device:TPU:0, one launch (start us, length us, event | category | flops | bytes accessed | tf_op | source)
XLA Modules:
  0.0 120.7 jit_solution(8492485326082151080)
XLA Ops:
  0.6 0.0 copy-start
  0.6 0.0 copy-start.11
  0.7 0.0 copy-start.12
  0.7 0.1 eq.50
  0.8 0.8 fusion.46
  1.5 0.1 convolution_select_fusion
  1.7 0.1 bitcast_compare_fusion
  1.8 1.7 %convolution_convert_fusion.5 = bf16[320,256]{1,0:T(8,128)(2,1)} fusion(pred[320,128]{1,0:T(32,128)(4,1)S(1)} %bitcast_compare_fusion, bf16[128,256]{1,0:T(8,128)(2,1)} %param.9), kind=kOutput, calls=%fused_computation.20 | convolution fusion | flops 21053440 | bytes 270336 | tf_op jit(solution)/shard_map/dot_general | solution.py:64
  3.5 7.3 %all-to-all-start.1 = ((bf16[8,40,256]{2,1,0:T(8,128)(2,1)}), bf16[8,40,256]{2,1,0:T(8,128)(2,1)S(1)}, u32[]{:S(2)}, u32[]{:S(2)}) async-start(bf16[8,40,256]{2,1,0:T(8,128)(2,1)} %bitcast.6), calls=%async_computation.1 | async-start | bytes 327680 | tf_op jit(solution)/shard_map/all_to_all | solution.py:18
  10.8 6.0 %all_gather.3 = bf16[128,1024]{1,0:T(8,128)(2,1)S(1)} all-gather(bf16[128,256]{1,0:T(8,128)(2,1)} %param.10), channel_id=1, replica_groups=mesh['ep'=8,'tp'=4] {'tp'}, dimensions={1}, use_global_device_ids=true | all-gather | bytes 327680 | tf_op jit(solution)/shard_map/all_gather | solution.py:68
  16.8 0.3 convolution_convert_fusion.3
  17.1 0.0 copy-done.12
  17.2 0.2 fusion.27
  17.3 0.9 pad_maximum_fusion.1
  18.3 0.1 all-to-all-done.1
  18.4 5.9 %all-to-all-start = ((bf16[8,40,1152]{2,1,0:T(8,128)(2,1)}), bf16[8,40,1152]{2,1,0:T(8,128)(2,1)}, u32[]{:S(2)}, u32[]{:S(2)}) async-start(bf16[8,40,1152]{2,1,0:T(8,128)(2,1)} %pad_maximum_fusion.1), calls=%async_computation | async-start | bytes 1474560 | tf_op jit(solution)/shard_map/all_to_all | solution.py:18
  24.3 0.1 collective-permute-start
  24.3 4.7 %collective-permute-done = bf16[320,256]{1,0:T(8,128)(2,1)S(1)} collective-permute-done((bf16[320,256]{1,0:T(8,128)(2,1)S(1)}, bf16[320,256]{1,0:T(8,128)(2,1)S(1)}, u32[]{:S(2)}, u32[]{:S(2)}) %collective-permute-start) | collective-permute-done | bytes 163872 | tf_op jit(solution)/shard_map/ppermute | solution.py:36
  29.0 0.0 collective-permute-start.1
  29.0 0.1 broadcast_in_dim.106
  29.1 4.6 %collective-permute-done.1 = bf16[320,256]{1,0:T(8,128)(2,1)S(1)} collective-permute-done((bf16[320,256]{1,0:T(8,128)(2,1)S(1)}, bf16[320,256]{1,0:T(8,128)(2,1)S(1)}, u32[]{:S(2)}, u32[]{:S(2)}) %collective-permute-start.1) | collective-permute-done | bytes 163872 | tf_op jit(solution)/shard_map/ppermute | solution.py:36
  33.7 0.0 collective-permute-start.2
  33.8 4.7 %collective-permute-done.2 = bf16[320,256]{1,0:T(8,128)(2,1)S(1)} collective-permute-done((bf16[320,256]{1,0:T(8,128)(2,1)S(1)}, bf16[320,256]{1,0:T(8,128)(2,1)S(1)}, u32[]{:S(2)}, u32[]{:S(2)}) %collective-permute-start.2) | collective-permute-done | bytes 163872 | tf_op jit(solution)/shard_map/ppermute | solution.py:36
  38.5 0.0 copy-start.2
  38.5 0.0 copy-start.1
  38.5 1.7 %fusion.5 = f32[320,704]{1,0:T(8,128)} fusion(bf16[320,1024]{1,0:T(8,128)(2,1)S(1)} %constant_dynamic-update-slice_fusion, bf16[1,1024,704]{1,2,0:T(8,128)(2,1)S(1)} %copy-done), kind=kOutput, calls=%fused_computation.8 | convolution fusion | flops 461373440 | bytes 2998272 | tf_op jit(solution)/shard_map/dot_general | solution.py:88
  40.2 1.7 %fusion.9 = f32[320,704]{1,0:T(8,128)} fusion(bf16[320,1024]{1,0:T(8,128)(2,1)S(1)} %constant_dynamic-update-slice_fusion, bf16[1,1024,704]{1,2,0:T(8,128)(2,1)S(1)} %copy-done.1), kind=kOutput, calls=%fused_computation.12 | convolution fusion | flops 461373440 | bytes 2998272 | tf_op jit(solution)/shard_map/dot_general | solution.py:89
  41.9 2.0 %all-to-all-done = bf16[8,40,1152]{2,1,0:T(8,128)(2,1)} async-done(((bf16[8,40,1152]{2,1,0:T(8,128)(2,1)}), bf16[8,40,1152]{2,1,0:T(8,128)(2,1)}, u32[]{:S(2)}, u32[]{:S(2)}) %all-to-all-start) | async-done | bytes 737312 | tf_op jit(solution)/shard_map/all_to_all | solution.py:18
  44.0 1.0 convert_reduce_fusion.1
  45.0 3.3 %multiply_reduce_fusion.1 = (f32[320]{0:T(512)S(1)}, bf16[320,704]{1,0:T(8,128)(2,1)S(1)}, bf16[320,704]{1,0:T(8,128)(2,1)S(1)}) fusion(f32[320,704]{1,0:T(8,128)} %fusion.9, f32[320,704]{1,0:T(8,128)} %fusion.5, f32[320]{0:T(512)S(1)} %convert_reduce_fusion.1, bf16[1,704,1024]{2,1,0:T(8,128)(2,1)} %param.15, bf16[320,1152]{1,0:T(8,128)(2,1)} %bitcast.4), kind=kOutput, calls=%fused_computation.29 | convolution fusion | flops 465653440 | bytes 4966912 | tf_op jit(solution)/shard_map/dot_general | solution.py:94
  48.3 0.7 fusion.3
  49.0 0.1 copy-done.15
  49.0 0.2 copy-done.7
  49.2 0.7 fusion.16
  49.9 0.0 copy-start.9
  49.9 0.9 copy.45
  50.8 3.6 %all-to-all-start.2 = ((bf16[320,4,256]{2,0,1:T(8,128)(2,1)}), bf16[320,4,256]{2,0,1:T(8,128)(2,1)S(1)}, u32[]{:S(2)}, u32[]{:S(2)}) async-start(bf16[320,4,256]{2,0,1:T(8,128)(2,1)} %bitcast.76), calls=%async_computation.2 | async-start | bytes 1310720 | tf_op jit(solution)/shard_map/all_to_all | solution.py:106
  54.4 0.0 copy-done.9
  54.5 0.1 copy.37
  54.6 10.1 %all-to-all-done.2 = bf16[320,4,256]{2,0,1:T(8,128)(2,1)S(1)} async-done(((bf16[320,4,256]{2,0,1:T(8,128)(2,1)}), bf16[320,4,256]{2,0,1:T(8,128)(2,1)S(1)}, u32[]{:S(2)}, u32[]{:S(2)}) %all-to-all-start.2) | async-done | bytes 655392 | tf_op jit(solution)/shard_map/all_to_all | solution.py:106
  64.6 0.8 reduce_sum.95
  65.4 4.0 %all-to-all-start.3 = ((bf16[8,40,256]{2,1,0:T(8,128)(2,1)}), bf16[8,40,256]{2,1,0:T(8,128)(2,1)S(1)}, u32[]{:S(2)}, u32[]{:S(2)}) async-start(bf16[8,40,256]{2,1,0:T(8,128)(2,1)} %bitcast.10), calls=%async_computation.3 | async-start | bytes 327680 | tf_op jit(solution)/shard_map/all_to_all | solution.py:18
  69.4 0.3 convolution_convert_fusion.4
  69.8 1.1 pad_maximum_fusion
  70.9 6.1 %all-to-all-done.3 = bf16[8,40,256]{2,1,0:T(8,128)(2,1)S(1)} async-done(((bf16[8,40,256]{2,1,0:T(8,128)(2,1)}), bf16[8,40,256]{2,1,0:T(8,128)(2,1)S(1)}, u32[]{:S(2)}, u32[]{:S(2)}) %all-to-all-start.3) | async-done | bytes 163872 | tf_op jit(solution)/shard_map/all_to_all | solution.py:18
  76.9 0.7 copy-done.4
  77.6 3.6 %all-to-all-start.4 = ((bf16[8,512,128]{1,2,0:T(8,128)(2,1)}), bf16[8,512,128]{1,2,0:T(8,128)(2,1)S(1)}, u32[]{:S(2)}, u32[]{:S(2)}) async-start(bf16[8,512,128]{1,2,0:T(8,128)(2,1)} %pad_maximum_fusion), calls=%async_computation.4 | async-start | bytes 2097152 | tf_op jit(solution)/shard_map/all_to_all | solution.py:18
  81.2 1.4 %fusion.55 = f32[256,1024]{0,1:T(8,128)} fusion(bf16[128,256]{1,0:T(8,128)(2,1)S(1)} %copy-done.6, bf16[128,1024]{1,0:T(8,128)(2,1)S(1)} %all_gather.3), kind=kOutput, calls=%fused_computation.88 | convolution fusion | flops 67108864 | bytes 1376256 | tf_op jit(solution)/shard_map/reshape | solution.py:110
  82.5 3.2 %fusion = bf16[1,1024,704]{1,2,0:T(8,128)(2,1)} fusion(bf16[320,1024]{1,0:T(8,128)(2,1)S(1)} %copy-done.3, bf16[320,704]{1,0:T(8,128)(2,1)} %copy-done.15), kind=kOutput, calls=%fused_computation.3 | convolution fusion | flops 462094336 | bytes 2547712 | tf_op jit(solution)/shard_map/dot_general | solution.py:123
  85.7 2.1 %fusion.1 = bf16[1,1024,704]{1,2,0:T(8,128)(2,1)} fusion(bf16[320,1024]{1,0:T(8,128)(2,1)S(1)} %copy-done.3, bf16[320,704]{1,0:T(8,128)(2,1)S(1)} %copy-done.8), kind=kOutput, calls=%fused_computation.4 | convolution fusion | flops 462094336 | bytes 2547712 | tf_op jit(solution)/shard_map/dot_general | solution.py:124
  87.8 3.3 %fusion.2 = bf16[1,704,1024]{2,1,0:T(8,128)(2,1)} fusion(bf16[320,1152]{1,0:T(8,128)(2,1)} %bitcast.4, f32[320]{0:T(512)S(1)} %convert_reduce_fusion.1, f32[320,704]{1,0:T(8,128)S(1)} %copy-done.14, f32[320,704]{1,0:T(8,128)S(1)} %copy-done.13), kind=kOutput, calls=%fused_computation.5 | convolution fusion | flops 463671296 | bytes 3900672 | tf_op jit(solution)/shard_map/dot_general | solution.py:125
  91.1 0.0 copy-done.5
  91.1 0.3 convolution_bitcast_fusion
  91.4 14.3 %all-to-all-done.4 = bf16[8,512,128]{1,2,0:T(8,128)(2,1)S(1)} async-done(((bf16[8,512,128]{1,2,0:T(8,128)(2,1)}), bf16[8,512,128]{1,2,0:T(8,128)(2,1)S(1)}, u32[]{:S(2)}, u32[]{:S(2)}) %all-to-all-start.4) | async-done | bytes 1048608 | tf_op jit(solution)/shard_map/all_to_all | solution.py:18
  105.7 1.5 %convert_reduce_fusion = (f32[256,128]{0,1:T(8,128)S(1)}, f32[8,128]{1,0:T(8,128)S(1)}) fusion(bf16[8,512,128]{1,2,0:T(8,128)(2,1)S(1)} %all-to-all-done.4, f32[8,256,128]{1,2,0:T(8,128)} %bitcast.78), kind=kLoop, calls=%fused_computation.26 | loop fusion | flops 1276928 | bytes 2232320 | tf_op jit(solution)/shard_map/reduce_sum | solution.py:84
  107.2 0.1 broadcast_in_dim.110
  107.3 0.8 broadcast_in_dim.112
  108.0 2.9 %all-to-all-start.5 = ((f32[32,1,1064]{2,1,0:T(1,128)}), f32[32,1,1064]{2,1,0:T(1,128)S(1)}, u32[]{:S(2)}, u32[]{:S(2)}) async-start(f32[32,1,1064]{2,1,0:T(1,128)} %broadcast_in_dim.112), calls=%async_computation.5 | async-start | bytes 294912 | tf_op jit(solution)/shard_map/all_to_all | solution.py:18
  111.0 0.8 copy.39
  111.8 0.9 fusion.19
  112.6 6.7 %all-to-all-done.5 = f32[32,1,1064]{2,1,0:T(1,128)S(1)} async-done(((f32[32,1,1064]{2,1,0:T(1,128)}), f32[32,1,1064]{2,1,0:T(1,128)S(1)}, u32[]{:S(2)}, u32[]{:S(2)}) %all-to-all-start.5) | async-done | bytes 136224 | tf_op jit(solution)/shard_map/all_to_all | solution.py:18
  119.4 0.1 fusion.29
  119.6 0.6 select_reduce_fusion
  120.1 0.6 broadcast_multiply_fusion.1
  (38 shorter events, 0.3 us)
Async XLA Ops:
  0.6 37.9 %copy-start = (bf16[1,1024,704]{1,2,0:T(8,128)(2,1)S(1)}, bf16[1,1024,704]{1,2,0:T(8,128)(2,1)}, u32[]{:S(2)}) copy-start(bf16[1,1024,704]{1,2,0:T(8,128)(2,1)} %param.13) | copy-start | bytes 4325380
  0.6 16.5 %copy-start.11 = (s32[128,2]{0,1:T(2,128)S(1)}, s32[128,2]{0,1:T(2,128)}, u32[]{:S(2)}) copy-start(s32[128,2]{0,1:T(2,128)} %param.11) | copy-start | bytes 3076
  0.7 16.4 %copy-start.12 = (bf16[128,2]{0,1:T(2,128)(2,1)S(1)}, bf16[128,2]{0,1:T(2,128)(2,1)}, u32[]{:S(2)}) copy-start(bf16[128,2]{0,1:T(2,128)(2,1)} %param.12) | copy-start | bytes 1540
  3.5 14.8 %all-to-all-start.1 = ((bf16[8,40,256]{2,1,0:T(8,128)(2,1)}), bf16[8,40,256]{2,1,0:T(8,128)(2,1)S(1)}, u32[]{:S(2)}, u32[]{:S(2)}) async-start(bf16[8,40,256]{2,1,0:T(8,128)(2,1)} %bitcast.6), calls=%async_computation.1 | async-start | bytes 327680 | tf_op jit(solution)/shard_map/all_to_all | solution.py:18
  18.4 25.6 %all-to-all-start = ((bf16[8,40,1152]{2,1,0:T(8,128)(2,1)}), bf16[8,40,1152]{2,1,0:T(8,128)(2,1)}, u32[]{:S(2)}, u32[]{:S(2)}) async-start(bf16[8,40,1152]{2,1,0:T(8,128)(2,1)} %pad_maximum_fusion.1), calls=%async_computation | async-start | bytes 1474560 | tf_op jit(solution)/shard_map/all_to_all | solution.py:18
  24.3 4.7 %collective-permute-start = (bf16[320,256]{1,0:T(8,128)(2,1)S(1)}, bf16[320,256]{1,0:T(8,128)(2,1)S(1)}, u32[]{:S(2)}, u32[]{:S(2)}) collective-permute-start(bf16[320,256]{1,0:T(8,128)(2,1)S(1)} %bitcast.83), channel_id=1, source_target_pairs={{0,1},{1,2},{2,3},{3,0},{4,5},{5,6},{6,7},{7,4},{8,9},{9,10},{10,1... | collective-permute-start | bytes 491528 | tf_op jit(solution)/shard_map/ppermute | solution.py:36
  29.0 4.7 %collective-permute-start.1 = (bf16[320,256]{1,0:T(8,128)(2,1)S(1)}, bf16[320,256]{1,0:T(8,128)(2,1)S(1)}, u32[]{:S(2)}, u32[]{:S(2)}) collective-permute-start(bf16[320,256]{1,0:T(8,128)(2,1)S(1)} %collective-permute-done), channel_id=1, source_target_pairs={{0,1},{1,2},{2,3},{3,0},{4,5},{5,6},{6,7},{7,4},{8,9},{9,10},{10,1... | collective-permute-start | bytes 491528 | tf_op jit(solution)/shard_map/ppermute | solution.py:36
  33.7 4.7 %collective-permute-start.2 = (bf16[320,256]{1,0:T(8,128)(2,1)S(1)}, bf16[320,256]{1,0:T(8,128)(2,1)S(1)}, u32[]{:S(2)}, u32[]{:S(2)}) collective-permute-start(bf16[320,256]{1,0:T(8,128)(2,1)S(1)} %collective-permute-done.1), channel_id=1, source_target_pairs={{0,1},{1,2},{2,3},{3,0},{4,5},{5,6},{6,7},{7,4},{8,9},{9,10},{10,1... | collective-permute-start | bytes 491528 | tf_op jit(solution)/shard_map/ppermute | solution.py:36
  38.5 1.7 %copy-start.2 = (bf16[320,1024]{1,0:T(8,128)(2,1)}, bf16[320,1024]{1,0:T(8,128)(2,1)S(1)}, u32[]{:S(2)}) copy-start(bf16[320,1024]{1,0:T(8,128)(2,1)S(1)} %constant_dynamic-update-slice_fusion) | copy-start | bytes 1966084
  38.5 1.7 %copy-start.1 = (bf16[1,1024,704]{1,2,0:T(8,128)(2,1)S(1)}, bf16[1,1024,704]{1,2,0:T(8,128)(2,1)}, u32[]{:S(2)}) copy-start(bf16[1,1024,704]{1,2,0:T(8,128)(2,1)} %param.14) | copy-start | bytes 4325380
  48.3 0.8 copy-start.15
  48.3 1.0 copy-start.7
  49.9 4.5 %copy-start.9 = (bf16[256,128]{1,0:T(8,128)(2,1)S(1)}, bf16[256,128]{1,0:T(8,128)(2,1)}, u32[]{:S(2)}) copy-start(bf16[256,128]{1,0:T(8,128)(2,1)} %param.16) | copy-start | bytes 196612
  50.8 18.6 %copy-start.6 = (bf16[128,256]{1,0:T(8,128)(2,1)S(1)}, bf16[128,256]{1,0:T(8,128)(2,1)}, u32[]{:S(2)}) copy-start(bf16[128,256]{1,0:T(8,128)(2,1)} %param.9) | copy-start | bytes 196612
  50.8 18.6 %copy-start.10 = (f32[1024]{0:T(1024)S(1)}, f32[1024]{0:T(1024)}, u32[]{:S(2)}) copy-start(f32[1024]{0:T(1024)} %param.17) | copy-start | bytes 12292
  50.8 13.8 %all-to-all-start.2 = ((bf16[320,4,256]{2,0,1:T(8,128)(2,1)}), bf16[320,4,256]{2,0,1:T(8,128)(2,1)S(1)}, u32[]{:S(2)}, u32[]{:S(2)}) async-start(bf16[320,4,256]{2,0,1:T(8,128)(2,1)} %bitcast.76), calls=%async_computation.2 | async-start | bytes 1310720 | tf_op jit(solution)/shard_map/all_to_all | solution.py:106
  65.4 11.5 %all-to-all-start.3 = ((bf16[8,40,256]{2,1,0:T(8,128)(2,1)}), bf16[8,40,256]{2,1,0:T(8,128)(2,1)S(1)}, u32[]{:S(2)}, u32[]{:S(2)}) async-start(bf16[8,40,256]{2,1,0:T(8,128)(2,1)} %bitcast.10), calls=%async_computation.3 | async-start | bytes 327680 | tf_op jit(solution)/shard_map/all_to_all | solution.py:18
  70.9 11.7 %copy-start.3 = (bf16[320,1024]{1,0:T(8,128)(2,1)S(1)}, bf16[320,1024]{1,0:T(8,128)(2,1)}, u32[]{:S(2)}) copy-start(bf16[320,1024]{1,0:T(8,128)(2,1)} %copy-done.2) | copy-start | bytes 1966084
  76.9 0.7 copy-start.4
  77.6 28.1 %all-to-all-start.4 = ((bf16[8,512,128]{1,2,0:T(8,128)(2,1)}), bf16[8,512,128]{1,2,0:T(8,128)(2,1)S(1)}, u32[]{:S(2)}, u32[]{:S(2)}) async-start(bf16[8,512,128]{1,2,0:T(8,128)(2,1)} %pad_maximum_fusion), calls=%async_computation.4 | async-start | bytes 2097152 | tf_op jit(solution)/shard_map/all_to_all | solution.py:18
  82.5 3.2 %copy-start.8 = (bf16[320,704]{1,0:T(8,128)(2,1)S(1)}, bf16[320,704]{1,0:T(8,128)(2,1)}, u32[]{:S(2)}) copy-start(bf16[320,704]{1,0:T(8,128)(2,1)} %copy-done.7) | copy-start | bytes 1351684
  85.7 2.1 %copy-start.13 = (f32[320,704]{1,0:T(8,128)S(1)}, f32[320,704]{1,0:T(8,128)}, u32[]{:S(2)}) copy-start(f32[320,704]{1,0:T(8,128)} %fusion.5) | copy-start | bytes 2703364
  85.7 2.1 %copy-start.14 = (f32[320,704]{1,0:T(8,128)S(1)}, f32[320,704]{1,0:T(8,128)}, u32[]{:S(2)}) copy-start(f32[320,704]{1,0:T(8,128)} %fusion.9) | copy-start | bytes 2703364
  87.8 3.3 %copy-start.5 = (bf16[8,40,256]{2,1,0:T(8,128)(2,1)S(1)}, bf16[8,40,256]{2,1,0:T(8,128)(2,1)}, u32[]{:S(2)}) copy-start(bf16[8,40,256]{2,1,0:T(8,128)(2,1)} %copy-done.4) | copy-start | bytes 491524
  108.0 11.3 %all-to-all-start.5 = ((f32[32,1,1064]{2,1,0:T(1,128)}), f32[32,1,1064]{2,1,0:T(1,128)S(1)}, u32[]{:S(2)}, u32[]{:S(2)}) async-start(f32[32,1,1064]{2,1,0:T(1,128)} %broadcast_in_dim.112), calls=%async_computation.5 | async-start | bytes 294912 | tf_op jit(solution)/shard_map/all_to_all | solution.py:18
